TPU v7x, 32 devices: a whole 2x2x4 slice. The times are simulated.
32 devices in a mesh: ep: 32 (over z, y, x, core).
Axes of the slice: x: 2, y: 2, z: 4, core: 2. Of those that a mesh axis runs over, the one named last changes fastest.
Arguments:
- hidden: bfloat16 [1024, 2048], P('ep'), may hold values from -6 to 6
- cache_keys: bfloat16 [1024, 1024, 128], P('ep'), may hold values from -512 to 512
- cache_values: bfloat16 [1024, 1024, 128], P('ep'), may hold values from -6 to 6
- lengths: int32 [1024], P('ep'), may hold values from 1 to 1024
- first_gain: float32 [2048], replicated, may hold values from 0.1 to 1.9
- query_weight: bfloat16 [2048, 1024], replicated, may hold values from -0.125 to 0.125
- key_weight: bfloat16 [2048, 128], replicated, may hold values from -0.125 to 0.125
- value_weight: bfloat16 [2048, 128], replicated, may hold values from -0.125 to 0.125
- mixing: float32 [8], replicated, may hold values from 0.3 to 0.8
- head_gain: float32 [128], replicated, may hold values from 0.1 to 1.9
- out_weight: bfloat16 [1024, 2048], replicated, may hold values from -0.1875 to 0.1875
- second_gain: float32 [2048], replicated, may hold values from 0.1 to 1.9
- routes: int32 [1024, 4], P('ep'), may hold values from 0 to 15, as said below
- route_weight: float32 [1024, 4], P('ep'), may hold values from 0.05 to 1
- expert_gate: bfloat16 [32, 2048, 256], P('ep'), may hold values from -0.125 to 0.125
- expert_up: bfloat16 [32, 2048, 256], P('ep'), may hold values from -0.125 to 0.125
- expert_down: bfloat16 [32, 256, 2048], P('ep'), may hold values from -0.25 to 0.25
Outputs:
- layer_out: bfloat16 [1024, 2048], P('ep')
- new_key: bfloat16 [1024, 128], P('ep')
- new_value: bfloat16 [1024, 128], P('ep')
Inputs may be any that keep to these rules, and one draw needn't show every extreme that they name: `routes`: each row names 4 different experts of one group, that is of one block of 4 consecutive numbers. Among the rows of one device, two rows name the same set of experts or disjoint sets, and no expert is named by more than 16 rows; one and the same expert is named by exactly 16 rows on every device.
All inputs are finite; a program needn't handle non-finite values.
Results may differ from a plain program's by a relative error of at most 0.025.
Values may be sent and summed in bfloat16 or wider, within the bound.
A program may use at most 128 MiB of HBM per device.

v0:
```python
import functools
import math

import jax
import jax.numpy as jnp
from jax import lax
from jax.experimental import pallas as pl
from jax.experimental.pallas import tpu as pltpu
from jax.sharding import PartitionSpec as P

D = 2048
HEADS = 8
DK = 64
DV = 128
EXP_SPLIT = 2
TOP_K = 4
GROUPS = 4
SIDE = 64


epsilon = 1e-06


def column(row):
    size = row.shape[1]
    down = lax.broadcasted_iota(jnp.int32, (size, size), 0)
    across = lax.broadcasted_iota(jnp.int32, (size, size), 1)
    return jnp.sum(jnp.where(down == across, row, jnp.zeros_like(row)), axis=1, keepdims=True)


def front_kernel(height, each, lengths, hidden, keys, values, first_gain, query_weight, key_weight, value_weight,
                 mixing, head_gain, out_weight, second_gain, routes, route_weight,
                 residual, new_key, new_value, pack, unpick,
                 key_buf, value_buf, query_buf, kv_buf, out_buf, queries, heads, fresh, sems, key_sems, value_sems):
    count, width = hidden.shape
    span = keys.shape[1]
    groups = key_sems.shape[0]
    batch = count // groups
    low = jnp.bfloat16
    loads = [
        pltpu.make_async_copy(query_weight, query_buf, sems.at[0]),
        pltpu.make_async_copy(key_weight, kv_buf.at[0], sems.at[1]),
        pltpu.make_async_copy(value_weight, kv_buf.at[1], sems.at[2]),
        pltpu.make_async_copy(out_weight, out_buf, sems.at[3]),
    ]

    def stream(step):
        at = pl.ds(step * batch, batch)
        return (
            pltpu.make_async_copy(keys.at[at], key_buf.at[at], key_sems.at[step]),
            pltpu.make_async_copy(values.at[at], value_buf.at[at], value_sems.at[step]),
        )

    for copy in loads[:3]:
        copy.start()

    def begin(step, carry):
        for copy in stream(step):
            copy.start()
        return carry

    lax.fori_loop(0, groups, begin, 0)
    loads[3].start()

    entry = hidden[...].astype(jnp.float32)
    factor = lax.rsqrt(jnp.mean(entry * entry, axis=-1, keepdims=True) + epsilon)
    normed = (entry * factor * first_gain[...]).astype(low)
    lane = lax.broadcasted_iota(jnp.int32, (count, 2 * DK), 1)
    loads[0].wait()
    query = jnp.dot(normed, query_buf[...], preferred_element_type=jnp.float32)
    query = query.astype(low).astype(jnp.float32)
    for head in range(HEADS):
        block = query[:, head * 2 * DK : (head + 1) * 2 * DK]
        queries[:, head, :] = jnp.where(lane < DK, block, 0.0)
        queries[:, HEADS + head, :] = jnp.where(lane < DK, 0.0, block)
    for index, result in ((0, new_key), (1, new_value)):
        loads[1 + index].wait()
        made = jnp.dot(normed, kv_buf[index], preferred_element_type=jnp.float32).astype(low)
        result[...] = made
        fresh[index] = made.astype(jnp.float32)

    position = lax.broadcasted_iota(jnp.int32, (1, span), 1)

    mixes = column(mixing[...])

    def attend(step, carry):
        for copy in stream(step):
            copy.wait()
        rows = []
        for offset in range(batch):
            s = step * batch + offset
            wide = queries[s]
            own_key = fresh[0, pl.ds(s, 1), :]
            own_value = fresh[1, pl.ds(s, 1), :]
            scores = lax.dot_general(
                wide.astype(low),
                key_buf[s],
                (((1,), (1,)), ((), ())),
                preferred_element_type=jnp.float32,
            ) * DK ** (-0.5)
            own = jnp.sum(wide * own_key, axis=-1, keepdims=True) * DK ** (-0.5)
            scores = jnp.where(position < lengths[s], scores, -jnp.inf)
            highest = jnp.maximum(jnp.max(scores, axis=-1, keepdims=True), own)
            weights = jnp.exp(scores - highest)
            own = jnp.exp(own - highest)
            inverse = 1.0 / (jnp.sum(weights, axis=-1, keepdims=True) + own)
            first, second = inverse[:HEADS], inverse[HEADS:] * mixes
            contrast = (weights[:HEADS] * first - weights[HEADS:] * second).astype(low)
            own = (own[:HEADS] * first - own[HEADS:] * second).astype(low).astype(jnp.float32)
            mixed = jnp.dot(contrast, value_buf[s], preferred_element_type=jnp.float32)
            mixed += own * own_value
            scale = lax.rsqrt(jnp.mean(mixed * mixed, axis=-1, keepdims=True) + epsilon)
            rows.append(mixed * scale * head_gain[...])
        for offset in range(batch):
            heads[step * batch + offset] = rows[offset]
        return carry

    lax.fori_loop(0, groups, attend, 0)

    joined = jnp.concatenate([heads[:, head, :] for head in range(HEADS)], axis=1).astype(low)
    loads[3].wait()
    update = jnp.dot(joined, out_buf[...], preferred_element_type=jnp.float32)
    kept = (hidden[...].astype(jnp.float32) + update).astype(low)
    residual[...] = kept
    kept = kept.astype(jnp.float32)
    factor = lax.rsqrt(jnp.mean(kept * kept, axis=-1, keepdims=True) + epsilon)
    inputs = (kept * factor * second_gain[...]).astype(low)

    group = column(routes[:1, :]) // each
    down = lax.broadcasted_iota(jnp.int32, (count, count), 0)
    across = lax.broadcasted_iota(jnp.int32, (count, count), 1)
    other = routes[:1, :] // each
    before = jnp.where((group == other) & (across < down), 1, 0)
    target = group * height + jnp.sum(before, axis=1, keepdims=True)
    slots = GROUPS * height
    chosen = target == lax.broadcasted_iota(jnp.int32, (count, slots), 1)
    chosen = jnp.where(chosen, 1.0, 0.0).astype(low)
    unpick[...] = chosen
    place = lax.broadcasted_iota(jnp.int32, (count, SIDE), 1)
    scale = jnp.zeros((count, SIDE), jnp.float32)
    for k in range(routes.shape[0]):
        inside = column(routes[k : k + 1, :]) - group * each
        scale += jnp.where(place == inside, column(route_weight[k : k + 1, :]), 0.0)
    high = scale.astype(low)
    side = jnp.concatenate([high, (scale - high.astype(jnp.float32)).astype(low)], axis=1)
    turned = (((0,), (0,)), ((), ()))
    packed = lax.dot_general(chosen, inputs, turned, preferred_element_type=jnp.float32)
    pack[:, :, :width] = packed.astype(low).reshape(GROUPS, height, width)
    packed = lax.dot_general(chosen, side, turned, preferred_element_type=jnp.float32)
    pack[:, :, width:] = packed.astype(low).reshape(GROUPS, height, 2 * SIDE)


def run_front(arrays, height, each):
    (hidden, cache_keys, cache_values, lengths, first_gain, query_weight, key_weight, value_weight,
     mixing, head_gain, out_weight, second_gain, routes, route_weight) = arrays
    count, width = hidden.shape
    low = jnp.bfloat16
    vmem = pl.BlockSpec(memory_space=pltpu.VMEM)
    anywhere = pl.BlockSpec(memory_space=pl.ANY)
    batch = 4 if count % 4 == 0 else 1
    groups = count // batch
    slots = GROUPS * height
    span = cache_keys.shape[1]
    flops = 2 * count * (2 * query_weight.size + 2 * key_weight.size + 24 * span * DV)
    moved = 2 * (cache_keys.size + cache_values.size + 2 * query_weight.size)
    return pl.pallas_call(
        functools.partial(front_kernel, height, each),
        out_shape=(
            jax.ShapeDtypeStruct((count, width), low),
            jax.ShapeDtypeStruct((count, 2 * DK), low),
            jax.ShapeDtypeStruct((count, DV), low),
            jax.ShapeDtypeStruct((GROUPS, height, width + 2 * SIDE), low),
            jax.ShapeDtypeStruct((count, slots), low),
        ),
        in_specs=[
            pl.BlockSpec(memory_space=pltpu.SMEM), vmem, anywhere, anywhere, vmem, anywhere,
            anywhere, anywhere, vmem, vmem, anywhere, vmem, vmem, vmem,
        ],
        out_specs=(vmem,) * 5,
        scratch_shapes=[
            pltpu.VMEM(cache_keys.shape, low),
            pltpu.VMEM(cache_values.shape, low),
            pltpu.VMEM(query_weight.shape, low),
            pltpu.VMEM((2, *key_weight.shape), low),
            pltpu.VMEM(out_weight.shape, low),
            pltpu.VMEM((count, 2 * HEADS, 2 * DK), jnp.float32),
            pltpu.VMEM((count, HEADS, DV), jnp.float32),
            pltpu.VMEM((2, count, DV), jnp.float32),
            pltpu.SemaphoreType.DMA((4,)),
            pltpu.SemaphoreType.DMA((groups,)),
            pltpu.SemaphoreType.DMA((groups,)),
        ],
        compiler_params=pltpu.CompilerParams(vmem_limit_bytes=63 * 1024 * 1024),
        cost_estimate=pl.CostEstimate(flops=flops, bytes_accessed=moved, transcendentals=0),
        name="front",
    )(
        lengths, hidden, cache_keys, cache_values, first_gain.reshape(1, -1), query_weight,
        key_weight, value_weight, mixing.reshape(1, -1), head_gain.reshape(1, -1), out_weight,
        second_gain.reshape(1, -1), routes.T, route_weight.T,
    )


def moe_kernel(dims, pack, gate_own, up_own, down_own, gate_other, up_other, down_other, residual, unpick, out,
               rows, part, first_a, send_a, second_a, first_b, send_b, second_b, final, back,
               gate, up, down, send_sems, recv_sems, local_sems):
    zs_count, ys, xs = dims
    me = lax.axis_index("ep")
    c = lax.rem(me, 2)
    x = lax.rem(me // 2, xs)
    y = lax.rem(me // (2 * xs), ys)
    z = me // (2 * xs * ys)

    def device(pz, py, px):
        return ((pz * ys + py) * xs + px) * 2 + c

    def slot(pz, py, px):
        return (pz * ys + py) * xs + px

    def zat(k):
        return lax.rem(z + k + zs_count, zs_count)

    def yat(k):
        return lax.rem(y + k + ys, ys)

    def xat(k):
        return lax.rem(x + k + xs, xs)

    used = []

    def send(src, dst, target):
        index = len(used)
        copy = pltpu.make_async_remote_copy(
            src_ref=src,
            dst_ref=dst,
            send_sem=send_sems.at[index],
            recv_sem=recv_sems.at[index],
            device_id=(target,),
            device_id_type=pl.DeviceIdType.MESH,
        )
        copy.start()
        used.append(copy)
        return copy

    weights = []
    for index, (src, dst) in enumerate(
        (
            (gate_own.at[0], gate.at[0]),
            (up_own.at[0], up.at[0]),
            (gate_other.at[0], gate.at[1]),
            (up_other.at[0], up.at[1]),
            (down_own.at[0], down.at[0]),
            (down_other.at[0], down.at[1]),
        )
    ):
        copy = pltpu.make_async_copy(src, dst, local_sems.at[index + 1])
        copy.start()
        weights.append(copy)

    barrier = pltpu.get_barrier_semaphore()
    peers = [device(zat(k), y, x) for k in range(1, zs_count)]
    peers += [device(z, yat(k), x) for k in range(1, ys)]
    peers += [device(z, y, xat(k)) for k in range(1, xs)]
    for peer in peers:
        pl.semaphore_signal(barrier, inc=1, device_id=(peer,), device_id_type=pl.DeviceIdType.MESH)
    pl.semaphore_wait(barrier, len(peers))

    mine = slot(z, y, x)
    own = pltpu.make_async_copy(pack.at[z], rows.at[mine], local_sems.at[0])
    own.start()
    arrive = {}
    for k in range(1, zs_count):
        arrive[k] = send(pack.at[zat(k)], rows.at[mine], device(zat(k), y, x))
    order = sorted(range(zs_count), key=lambda k: min(k, zs_count - k))
    along_x, along_y, pending = {}, {}, []
    for k in order:
        if k:
            arrive[k].wait_recv()
        else:
            own.wait()
        block = rows.at[slot(zat(-k), y, x)]

        def over_x():
            for j in range(1, xs):
                along_x[k, j] = send(block, block, device(z, y, xat(j)))

        def over_y():
            for i in range(1, ys):
                along_y[k, i] = send(block, block, device(z, yat(i), x))

        for step in (over_x, over_y) if k % 2 == 0 else (over_y, over_x):
            step()
    for k in order:
        pz = zat(-k)
        if k % 2 == 0:
            for j in range(1, xs):
                along_x.pop((k, j)).wait_recv()
                block = rows.at[slot(pz, y, xat(-j))]
                for i in range(1, ys):
                    pending.append(send(block, block, device(z, yat(i), x)))
        else:
            for i in range(1, ys):
                along_y.pop((k, i)).wait_recv()
                block = rows.at[slot(pz, yat(-i), x)]
                for j in range(1, xs):
                    pending.append(send(block, block, device(z, y, xat(j))))
    for copy in weights[:4]:
        copy.wait()
    for copy in (*along_x.values(), *along_y.values(), *pending):
        copy.wait_recv()
    for copy in weights[4:]:
        copy.wait()

    slots, height, width = rows.shape
    depth = part.shape[2]
    chosen = y * xs + x
    batch = max(1, min(slots, 256 // height))

    def apply(step, carry):
        at = pl.ds(step * batch, batch)
        flat = rows[at, :, :depth].reshape(batch * height, depth)
        side = rows[at, :, depth:].reshape(batch * height, width - depth).astype(jnp.float32)
        lane = lax.broadcasted_iota(jnp.int32, side.shape, 1)
        hit = lax.rem(lane, (width - depth) // 2) == chosen
        scale = jnp.sum(jnp.where(hit, side, 0.0), axis=1, keepdims=True)
        inner = []
        for half in range(2):
            left = jnp.dot(flat, gate[half], preferred_element_type=jnp.float32)
            right = jnp.dot(flat, up[half], preferred_element_type=jnp.float32)
            inner.append((left / (1.0 + jnp.exp(-left)) * right).astype(jnp.bfloat16))
        tile = 512
        for start in range(0, depth, tile):
            cols = slice(start, start + tile)
            total = jnp.dot(inner[0], down[0, :, cols], preferred_element_type=jnp.float32)
            total += jnp.dot(inner[1], down[1, :, cols], preferred_element_type=jnp.float32)
            part[at, :, cols] = (total * scale).astype(part.dtype).reshape(batch, height, tile)
        return carry

    lax.fori_loop(0, slots // batch, apply, 0)

    evens = [k for k in order if k % 2 == 0]
    odds = [k for k in order if k % 2 == 1]
    waits = {}
    for k in order:
        pz = zat(-k)
        index = k // 2
        if k % 2 == 0:
            waits[k] = [
                send(
                    part.at[pl.ds(slot(pz, yat(j), 0), xs)],
                    first_a.at[index, j - 1],
                    device(z, yat(j), x),
                )
                for j in range(1, ys)
            ]
        else:
            waits[k] = [
                send(
                    part.at[slot(pz, row, xat(j))],
                    first_b.at[index, j - 1, row],
                    device(z, y, xat(j)),
                )
                for j in range(1, xs)
                for row in range(ys)
            ]
    seconds = {}
    for k in order:
        pz = zat(-k)
        index = k // 2
        for copy in waits[k]:
            copy.wait_recv()
        seconds[k] = []
        if k % 2 == 0:
            for i in range(1, xs):
                total = part[slot(pz, y, xat(i))].astype(jnp.float32)
                for j in range(1, ys):
                    total += first_a[index, j - 1, xat(i)].astype(jnp.float32)
                send_a[index, i - 1] = total.astype(send_a.dtype)
                seconds[k].append(
                    send(send_a.at[index, i - 1], second_a.at[index, i - 1], device(z, y, xat(i)))
                )
        else:
            for i in range(1, ys):
                total = part[slot(pz, yat(i), x)].astype(jnp.float32)
                for j in range(1, xs):
                    total += first_b[index, j - 1, yat(i)].astype(jnp.float32)
                send_b[index, i - 1] = total.astype(send_b.dtype)
                seconds[k].append(
                    send(send_b.at[index, i - 1], second_b.at[index, i - 1], device(z, yat(i), x))
                )
    returns = []
    for k in sorted(order, key=lambda k: (k == 0, k)):
        pz = zat(-k)
        index = k // 2
        for copy in seconds[k]:
            copy.wait_recv()
        total = part[slot(pz, y, x)].astype(jnp.float32)
        if k % 2 == 0:
            for j in range(1, ys):
                total += first_a[index, j - 1, x].astype(jnp.float32)
            for i in range(1, xs):
                total += second_a[index, i - 1].astype(jnp.float32)
        else:
            for j in range(1, xs):
                total += first_b[index, j - 1, y].astype(jnp.float32)
            for i in range(1, ys):
                total += second_b[index, i - 1].astype(jnp.float32)
        if k:
            final[k - 1] = total.astype(final.dtype)
            returns.append(send(final.at[k - 1], back.at[z], device(pz, y, x)))
        else:
            back[z] = total.astype(back.dtype)
    for copy in returns:
        copy.wait_recv()
    filled = back[...].reshape(zs_count * height, depth)
    routed = jnp.dot(unpick[...], filled, preferred_element_type=jnp.float32)
    out[...] = (residual[...].astype(jnp.float32) + routed).astype(out.dtype)
    for copy in used:
        copy.wait_send()


def run_experts(pack, own, other, residual, unpick, devices):
    zs = GROUPS
    chips = devices // (2 * zs)
    xs = math.isqrt(chips)
    ys = chips // xs
    _, height, width = pack.shape
    depth = residual.shape[1]
    slots = devices // 2
    hidden = own[0].shape[2]
    evens, odds = (zs + 1) // 2, zs // 2
    low = jnp.bfloat16
    count = (zs - 1) * 2 + zs * (xs + ys - 2) + zs * (xs - 1) * (ys - 1)
    count += evens * (xs + ys - 2) + odds * ((xs - 1) * ys + ys - 1)
    vmem = pl.BlockSpec(memory_space=pltpu.VMEM)
    anywhere = pl.BlockSpec(memory_space=pl.ANY)
    return pl.pallas_call(
        functools.partial(moe_kernel, (zs, ys, xs)),
        out_shape=jax.ShapeDtypeStruct(residual.shape, low),
        in_specs=[vmem] + [anywhere] * 6 + [vmem] * 2,
        out_specs=vmem,
        scratch_shapes=[
            pltpu.VMEM((slots, height, width), low),
            pltpu.VMEM((slots, height, depth), low),
            pltpu.VMEM((evens, max(1, ys - 1), xs, height, depth), low),
            pltpu.VMEM((evens, max(1, xs - 1), height, depth), low),
            pltpu.VMEM((evens, max(1, xs - 1), height, depth), low),
            pltpu.VMEM((odds, max(1, xs - 1), ys, height, depth), low),
            pltpu.VMEM((odds, max(1, ys - 1), height, depth), low),
            pltpu.VMEM((odds, max(1, ys - 1), height, depth), low),
            pltpu.VMEM((zs - 1, height, depth), low),
            pltpu.VMEM((zs, height, depth), low),
            pltpu.VMEM((2, depth, hidden), low),
            pltpu.VMEM((2, depth, hidden), low),
            pltpu.VMEM((2, hidden, depth), low),
            pltpu.SemaphoreType.DMA((count,)),
            pltpu.SemaphoreType.DMA((count,)),
            pltpu.SemaphoreType.DMA((7,)),
        ],
        compiler_params=pltpu.CompilerParams(
            collective_id=0, has_side_effects=True, vmem_limit_bytes=63 * 1024 * 1024
        ),
        name="experts",
    )(pack, *own, *other, residual, unpick)


def per_device(
    hidden,
    cache_keys,
    cache_values,
    lengths,
    first_gain,
    query_weight,
    key_weight,
    value_weight,
    mixing,
    head_gain,
    out_weight,
    second_gain,
    routes,
    route_weight,
    expert_gate,
    expert_up,
    expert_down,
):
    count = hidden.shape[0]
    devices = lax.axis_size("ep")
    experts = devices // EXP_SPLIT
    capacity = max(2, 2 * count * TOP_K // experts)
    height = capacity * (experts // GROUPS) // TOP_K
    arrays = (
        hidden, cache_keys, cache_values, lengths, first_gain, query_weight, key_weight, value_weight,
        mixing, head_gain, out_weight, second_gain, routes, route_weight,
    )
    residual, new_key, new_value, pack, unpick = run_front(arrays, height, experts // GROUPS)
    swap = [(index, index ^ 1) for index in range(devices)]
    own = (expert_gate, expert_up, expert_down)
    other = tuple(lax.ppermute(array, "ep", swap) for array in own)
    layer_out = run_experts(pack, own, other, residual, unpick, devices)
    return (layer_out, new_key, new_value)


def solution(mesh):
    return jax.shard_map(
        per_device,
        mesh=mesh,
        in_specs=(
            P("ep", None),
            P("ep", None, None),
            P("ep", None, None),
            P("ep"),
            P(),
            P(),
            P(),
            P(),
            P(),
            P(),
            P(),
            P(),
            P("ep", None),
            P("ep", None),
            P("ep", None, None),
            P("ep", None, None),
            P("ep", None, None),
        ),
        out_specs=(P("ep", None), P("ep", None), P("ep", None)),
        check_vma=False,
    )
```

profile of v0, /device:TPU:0, one launch (start us, length us, event | category | flops | bytes accessed | tf_op | source)
XLA Modules:
  0.0 65.2 jit_solution(12956711584596310780)
XLA Ops:
  0.6 0.6 collective-permute-start
  1.2 0.1 collective-permute-start.1
  1.3 0.4 collective-permute-start.2
  1.7 20.7 %front.1 = (bf16[32,2048]{1,0:T(8,128)(2,1)}, bf16[32,128]{1,0:T(8,128)(2,1)}, bf16[32,128]{1,0:T(8,128)(2,1)}, bf16[4,16,2176]{2,1,0:T(8,128)(2,1)}, bf16[32,64]{1,0:T(8,128)(2,1)}) custom-call(s32[32]{0:T(128)} %lengths.1, bf16[32,2048]{1,0:T(8,128)(2,1)} %hidden.1, bf16[32,1024,128]{2,1,0:T(8,128)(2,1)} %keys.1, bf16[32,1024,128]{2,1,0:T(8,128)(2,1)} %values.1, ...), custom_call_target="tpu_custom_call" | custom-call | flops 503316480 | bytes 25165824 | tf_op jit(solution)/shard_map/front/pallas_call | solution.py:166
  22.4 0.0 collective-permute-done.gate_other
  22.4 0.0 collective-permute-done.1.up_other
  22.4 0.0 collective-permute-done.2.down_other
  22.4 41.2 %experts.1 = bf16[32,2048]{1,0:T(8,128)(2,1)} custom-call(bf16[4,16,2176]{2,1,0:T(8,128)(2,1)} %get-tuple-element.8.pack, bf16[1,2048,256]{2,1,0:T(8,128)(2,1)} %gate_own.1, bf16[1,2048,256]{2,1,0:T(8,128)(2,1)} %up_own.1, bf16[1,256,2048]{2,1,0:T(8,128)(2,1)} %down_own.1, bf16[1,2048,256]{2,1,0:T(8,128)(2,1)} %collective-permute-done.gate_other, ...), custom_call_target="tpu_custom_call" | custom-call | tf_op jit(solution)/shard_map/experts/pallas_call | solution.py:436
  63.6 1.6 %copy.21 = bf16[32,2048]{1,0:T(8,128)(2,1)} copy(bf16[32,2048]{1,0:T(8,128)(2,1)} %experts.1) | data formatting | bytes 262144
Async XLA Ops:
  0.6 21.8 %collective-permute-start = (bf16[1,2048,256]{2,1,0:T(8,128)(2,1)}, bf16[1,2048,256]{2,1,0:T(8,128)(2,1)}, u32[]{:S(2)}, u32[]{:S(2)}) collective-permute-start(bf16[1,2048,256]{2,1,0:T(8,128)(2,1)} %gate_own.1), channel_id=1, source_target_pairs={{0,1},{1,0},{2,3},{3,2},{4,5},{5,4},{6,7},{7,6},{8,9},{9,8},{10,11... | collective-permute-start | bytes 3145736 | tf_op jit(solution)/shard_map/ppermute | solution.py:497
  1.2 21.2 %collective-permute-start.1 = (bf16[1,2048,256]{2,1,0:T(8,128)(2,1)}, bf16[1,2048,256]{2,1,0:T(8,128)(2,1)}, u32[]{:S(2)}, u32[]{:S(2)}) collective-permute-start(bf16[1,2048,256]{2,1,0:T(8,128)(2,1)} %up_own.1), channel_id=1, source_target_pairs={{0,1},{1,0},{2,3},{3,2},{4,5},{5,4},{6,7},{7,6},{8,9},{9,8},{10,11... | collective-permute-start | bytes 3145736 | tf_op jit(solution)/shard_map/ppermute | solution.py:497
  1.3 21.2 %collective-permute-start.2 = (bf16[1,256,2048]{2,1,0:T(8,128)(2,1)}, bf16[1,256,2048]{2,1,0:T(8,128)(2,1)}, u32[]{:S(2)}, u32[]{:S(2)}) collective-permute-start(bf16[1,256,2048]{2,1,0:T(8,128)(2,1)} %down_own.1), channel_id=1, source_target_pairs={{0,1},{1,0},{2,3},{3,2},{4,5},{5,4},{6,7},{7,6},{8,9},{9,8},{10,11... | collective-permute-start | bytes 3145736 | tf_op jit(solution)/shard_map/ppermute | solution.py:497
where the time goes:
time: 65.4 us; the launch traced here: 65.2 us
  Pallas kernels  61.9 us (95%)
  local copies, waits for them, and re-layouts  1.57 us (2%)
  starting transfers between devices  1.07 us (2%)
  between operations  0.67 us (1%)
    pallas_call x1, Pallas kernels, run_experts(): pl.pallas_call(functools.partial(moe_kernel, (zs, ys, xs)), out_shape=jax...  41.2 us
    pallas_call x1, Pallas kernels, run_front(): pl.pallas_call(functools.partial(front_kernel, height, each), out_shape=(...  20.7 us
    unnamed x1, local copies, waits for them, and re-layouts  1.57 us
  transfers between devices with their start and end apart: 3, of which 0 were waited for; matrix products, arithmetic and copies ran while one was open for 0% of the time, Pallas kernels for 32%

commit v1 on v0

--- a/solution.py
+++ b/solution.py
@@ -31,7 +31,7 @@
 def front_kernel(height, each, lengths, hidden, keys, values, first_gain, query_weight, key_weight, value_weight,
                  mixing, head_gain, out_weight, second_gain, routes, route_weight,
                  residual, new_key, new_value, pack, unpick,
-                 key_buf, value_buf, query_buf, kv_buf, out_buf, queries, heads, fresh, sems, key_sems, value_sems):
+                 key_buf, value_buf, query_buf, kv_buf, out_buf, queries, heads, fresh, contrast, owns, sems, key_sems, value_sems):
     count, width = hidden.shape
     span = keys.shape[1]
     groups = key_sems.shape[0]
@@ -44,22 +44,29 @@
         pltpu.make_async_copy(out_weight, out_buf, sems.at[3]),
     ]
 
-    def stream(step):
+    def fetch(source, target, flags, step):
         at = pl.ds(step * batch, batch)
-        return (
-            pltpu.make_async_copy(keys.at[at], key_buf.at[at], key_sems.at[step]),
-            pltpu.make_async_copy(values.at[at], value_buf.at[at], value_sems.at[step]),
-        )
+        return pltpu.make_async_copy(source.at[at], target.at[at], flags.at[step])
+
+    def fetch_keys(step):
+        return fetch(keys, key_buf, key_sems, step)
+
+    def fetch_values(step):
+        return fetch(values, value_buf, value_sems, step)
 
     for copy in loads[:3]:
         copy.start()
 
-    def begin(step, carry):
-        for copy in stream(step):
-            copy.start()
+    def begin_keys(step, carry):
+        fetch_keys(step).start()
         return carry
 
-    lax.fori_loop(0, groups, begin, 0)
+    def begin_values(step, carry):
+        fetch_values(step).start()
+        return carry
+
+    lax.fori_loop(0, groups, begin_keys, 0)
+    lax.fori_loop(0, groups, begin_values, 0)
     loads[3].start()
 
     entry = hidden[...].astype(jnp.float32)
@@ -83,15 +90,12 @@
 
     mixes = column(mixing[...])
 
-    def attend(step, carry):
-        for copy in stream(step):
-            copy.wait()
-        rows = []
+    def weigh(step, carry):
+        fetch_keys(step).wait()
         for offset in range(batch):
             s = step * batch + offset
             wide = queries[s]
             own_key = fresh[0, pl.ds(s, 1), :]
-            own_value = fresh[1, pl.ds(s, 1), :]
             scores = lax.dot_general(
                 wide.astype(low),
                 key_buf[s],
@@ -105,17 +109,24 @@
             own = jnp.exp(own - highest)
             inverse = 1.0 / (jnp.sum(weights, axis=-1, keepdims=True) + own)
             first, second = inverse[:HEADS], inverse[HEADS:] * mixes
-            contrast = (weights[:HEADS] * first - weights[HEADS:] * second).astype(low)
+            contrast[s] = weights[:HEADS] * first - weights[HEADS:] * second
             own = (own[:HEADS] * first - own[HEADS:] * second).astype(low).astype(jnp.float32)
-            mixed = jnp.dot(contrast, value_buf[s], preferred_element_type=jnp.float32)
-            mixed += own * own_value
+            owns[s] = own * fresh[1, pl.ds(s, 1), :]
+        return carry
+
+    lax.fori_loop(0, groups, weigh, 0)
+
+    def mix(step, carry):
+        fetch_values(step).wait()
+        for offset in range(batch):
+            s = step * batch + offset
+            mixed = jnp.dot(contrast[s].astype(low), value_buf[s], preferred_element_type=jnp.float32)
+            mixed += owns[s]
             scale = lax.rsqrt(jnp.mean(mixed * mixed, axis=-1, keepdims=True) + epsilon)
-            rows.append(mixed * scale * head_gain[...])
-        for offset in range(batch):
-            heads[step * batch + offset] = rows[offset]
+            heads[s] = mixed * scale * head_gain[...]
         return carry
 
-    lax.fori_loop(0, groups, attend, 0)
+    lax.fori_loop(0, groups, mix, 0)
 
     joined = jnp.concatenate([heads[:, head, :] for head in range(HEADS)], axis=1).astype(low)
     loads[3].wait()
@@ -157,7 +168,7 @@
     low = jnp.bfloat16
     vmem = pl.BlockSpec(memory_space=pltpu.VMEM)
     anywhere = pl.BlockSpec(memory_space=pl.ANY)
-    batch = 4 if count % 4 == 0 else 1
+    batch = math.gcd(count, 16)
     groups = count // batch
     slots = GROUPS * height
     span = cache_keys.shape[1]
@@ -186,6 +197,8 @@
             pltpu.VMEM((count, 2 * HEADS, 2 * DK), jnp.float32),
             pltpu.VMEM((count, HEADS, DV), jnp.float32),
             pltpu.VMEM((2, count, DV), jnp.float32),
+            pltpu.VMEM((count, HEADS, span), jnp.float32),
+            pltpu.VMEM((count, HEADS, DV), jnp.float32),
             pltpu.SemaphoreType.DMA((4,)),
             pltpu.SemaphoreType.DMA((groups,)),
             pltpu.SemaphoreType.DMA((groups,)),

time: 65.4 us -> 56.2 us (0.86)
  Pallas kernels: 61.9 us -> 52.7 us
    pallas_call x1, Pallas kernels: 20.7 us -> 11.5 us  [run_front(): pl.pallas_call(functools.partial(front_kernel, height, each), out_shape=(...]
  transfers between devices with their start and end apart: 3 -> 3, of which waited for: 0 -> 0; matrix products, arithmetic and copies ran while one was open for 0% -> 0% of each run, Pallas kernels for 32% -> 21%
where the time goes in v1:
time: 56.2 us; the launch traced here: 56 us
  Pallas kernels  52.7 us (94%)
  local copies, waits for them, and re-layouts  1.57 us (3%)
  starting transfers between devices  1.07 us (2%)
  between operations  0.67 us (1%)
    pallas_call x1, Pallas kernels, run_experts(): pl.pallas_call(functools.partial(moe_kernel, (zs, ys, xs)), out_shape=jax...  41.2 us
    pallas_call x1, Pallas kernels, run_front(): pl.pallas_call(functools.partial(front_kernel, height, each), out_shape=(...  11.5 us
    unnamed x1, local copies, waits for them, and re-layouts  1.57 us
  transfers between devices with their start and end apart: 3, of which 0 were waited for; matrix products, arithmetic and copies ran while one was open for 0% of the time, Pallas kernels for 21%

profile of v1, /device:TPU:0, one launch (start us, length us, event | category | flops | bytes accessed | tf_op | source)
XLA Modules:
  0.0 56.0 jit_solution(7451102834316461193)
XLA Ops:
  0.6 0.6 collective-permute-start
  1.2 0.1 collective-permute-start.1
  1.3 0.4 collective-permute-start.2
  1.7 11.5 %front.1 = (bf16[32,2048]{1,0:T(8,128)(2,1)}, bf16[32,128]{1,0:T(8,128)(2,1)}, bf16[32,128]{1,0:T(8,128)(2,1)}, bf16[4,16,2176]{2,1,0:T(8,128)(2,1)}, bf16[32,64]{1,0:T(8,128)(2,1)}) custom-call(s32[32]{0:T(128)} %lengths.1, bf16[32,2048]{1,0:T(8,128)(2,1)} %hidden.1, bf16[32,1024,128]{2,1,0:T(8,128)(2,1)} %keys.1, bf16[32,1024,128]{2,1,0:T(8,128)(2,1)} %values.1, ...), custom_call_target="tpu_custom_call" | custom-call | flops 503316480 | bytes 25165824 | tf_op jit(solution)/shard_map/front/pallas_call | solution.py:177
  13.2 0.0 collective-permute-done.gate_other
  13.2 0.0 collective-permute-done.1.up_other
  13.2 0.0 collective-permute-done.2.down_other
  13.2 41.2 %experts.1 = bf16[32,2048]{1,0:T(8,128)(2,1)} custom-call(bf16[4,16,2176]{2,1,0:T(8,128)(2,1)} %get-tuple-element.8.pack, bf16[1,2048,256]{2,1,0:T(8,128)(2,1)} %gate_own.1, bf16[1,2048,256]{2,1,0:T(8,128)(2,1)} %up_own.1, bf16[1,256,2048]{2,1,0:T(8,128)(2,1)} %down_own.1, bf16[1,2048,256]{2,1,0:T(8,128)(2,1)} %collective-permute-done.gate_other, ...), custom_call_target="tpu_custom_call" | custom-call | tf_op jit(solution)/shard_map/experts/pallas_call | solution.py:449
  54.4 1.6 %copy.21 = bf16[32,2048]{1,0:T(8,128)(2,1)} copy(bf16[32,2048]{1,0:T(8,128)(2,1)} %experts.1) | data formatting | bytes 262144
Async XLA Ops:
  0.6 12.6 %collective-permute-start = (bf16[1,2048,256]{2,1,0:T(8,128)(2,1)}, bf16[1,2048,256]{2,1,0:T(8,128)(2,1)}, u32[]{:S(2)}, u32[]{:S(2)}) collective-permute-start(bf16[1,2048,256]{2,1,0:T(8,128)(2,1)} %gate_own.1), channel_id=1, source_target_pairs={{0,1},{1,0},{2,3},{3,2},{4,5},{5,4},{6,7},{7,6},{8,9},{9,8},{10,11... | collective-permute-start | bytes 3145736 | tf_op jit(solution)/shard_map/ppermute | solution.py:510
  1.2 12.0 %collective-permute-start.1 = (bf16[1,2048,256]{2,1,0:T(8,128)(2,1)}, bf16[1,2048,256]{2,1,0:T(8,128)(2,1)}, u32[]{:S(2)}, u32[]{:S(2)}) collective-permute-start(bf16[1,2048,256]{2,1,0:T(8,128)(2,1)} %up_own.1), channel_id=1, source_target_pairs={{0,1},{1,0},{2,3},{3,2},{4,5},{5,4},{6,7},{7,6},{8,9},{9,8},{10,11... | collective-permute-start | bytes 3145736 | tf_op jit(solution)/shard_map/ppermute | solution.py:510
  1.3 12.0 %collective-permute-start.2 = (bf16[1,256,2048]{2,1,0:T(8,128)(2,1)}, bf16[1,256,2048]{2,1,0:T(8,128)(2,1)}, u32[]{:S(2)}, u32[]{:S(2)}) collective-permute-start(bf16[1,256,2048]{2,1,0:T(8,128)(2,1)} %down_own.1), channel_id=1, source_target_pairs={{0,1},{1,0},{2,3},{3,2},{4,5},{5,4},{6,7},{7,6},{8,9},{9,8},{10,11... | collective-permute-start | bytes 3145736 | tf_op jit(solution)/shard_map/ppermute | solution.py:510

commit v2 on v1

v2 whole, which is shorter than its diff:
```python
import functools
import math

import jax
import jax.numpy as jnp
from jax import lax
from jax.experimental import pallas as pl
from jax.experimental.pallas import tpu as pltpu
from jax.sharding import PartitionSpec as P

D = 2048
HEADS = 8
DK = 64
DV = 128
EXP_SPLIT = 2
TOP_K = 4
GROUPS = 4
SIDE = 64
ORDER = ('s0', 'f0', 's1', 'f1', 's2', 'f2', 's3', 'f3', 'c2', 'c3', 'e2', 'c1', 'e3', 'c0', 'e1', 'e0')
STRAIGHT = (0, 1, 2, 3)
GATHER = (0, 1, 2, 3)


epsilon = 1e-06


def column(row):
    size = row.shape[1]
    down = lax.broadcasted_iota(jnp.int32, (size, size), 0)
    across = lax.broadcasted_iota(jnp.int32, (size, size), 1)
    return jnp.sum(jnp.where(down == across, row, jnp.zeros_like(row)), axis=1, keepdims=True)


def layer_kernel(dims, height, each, lengths, hidden_in, keys, values, first_gain_in, query_weight, key_weight,
                 value_weight, mixing_in, head_gain_in, out_weight, second_gain_in, routes_in, route_weight_in,
                 gate_own, up_own, down_own,
                 out, new_key, new_value,
                 hidden, first_gain, mixing, head_gain, second_gain, routes, route_weight,
                 key_buf, value_buf, query_buf, kv_buf, out_buf, queries, heads, fresh, contrast, owns,
                 pack, side_pack, residual, rows, sides, part_a, part_b, first_a, first_b, send_a, send_b,
                 second_a, second_b, direct, final, back, gate, up, down,
                 load_sems, key_sems, value_sems, send_sems, recv_sems):
    zs, ys, xs = dims
    count, width = hidden.shape
    half = width // 2
    span = keys.shape[1]
    groups = key_sems.shape[0]
    batch = count // groups
    low = jnp.bfloat16
    me = lax.axis_index("ep")
    c = lax.rem(me, 2)
    x = lax.rem(me // 2, xs)
    y = lax.rem(me // (2 * xs), ys)
    z = me // (2 * xs * ys)

    def device(pz, py, px):
        return ((pz * ys + py) * xs + px) * 2 + c

    def zat(i):
        flip = z
        if i % 2:
            flip = flip + 1 - 2 * lax.rem(flip, 2)
        if i // 2:
            flip = lax.rem(flip + 2, 4)
        return flip

    def yat(j):
        return lax.rem(y + j + ys, ys)

    def xat(j):
        return lax.rem(x + j + xs, xs)

    used = []

    def send(src, dst, target):
        index = len(used)
        copy = pltpu.make_async_remote_copy(
            src_ref=src,
            dst_ref=dst,
            send_sem=send_sems.at[index],
            recv_sem=recv_sems.at[index],
            device_id=(target,),
            device_id_type=pl.DeviceIdType.MESH,
        )
        copy.start()
        used.append(copy)
        return copy

    others = [
        (i, j, k) for i in range(zs) for j in range(ys) for k in range(xs) if (i, j, k) != (0, 0, 0)
    ]
    sibling = me + 1 - 2 * c
    barrier = pltpu.get_barrier_semaphore()
    for i, j, k in others:
        pl.semaphore_signal(
            barrier, inc=1, device_id=(device(zat(i), yat(j), xat(k)),), device_id_type=pl.DeviceIdType.MESH
        )
    pl.semaphore_signal(barrier, inc=1, device_id=(sibling,), device_id_type=pl.DeviceIdType.MESH)

    moves = []
    for src, dst in (
        (hidden_in, hidden), (first_gain_in, first_gain), (routes_in, routes), (route_weight_in, route_weight),
        (mixing_in, mixing), (head_gain_in, head_gain), (second_gain_in, second_gain),
        (query_weight, query_buf), (key_weight, kv_buf.at[0]), (value_weight, kv_buf.at[1]),
        (out_weight, out_buf), (gate_own.at[0], gate.at[0]), (up_own.at[0], up.at[0]), (down_own.at[0], down.at[0]),
    ):
        moves.append(pltpu.make_async_copy(src, dst, load_sems.at[len(moves)]))
    small, query_move, kv_moves, out_move, own_moves = moves[:7], moves[7], moves[8:10], moves[10], moves[11:]

    def fetch(source, target, flags, step):
        at = pl.ds(step * batch, batch)
        return pltpu.make_async_copy(source.at[at], target.at[at], flags.at[step])

    def fetch_keys(step):
        return fetch(keys, key_buf, key_sems, step)

    def fetch_values(step):
        return fetch(values, value_buf, value_sems, step)

    for copy in (*small, query_move, *kv_moves):
        copy.start()

    def begin_keys(step, carry):
        fetch_keys(step).start()
        return carry

    def begin_values(step, carry):
        fetch_values(step).start()
        return carry

    lax.fori_loop(0, groups, begin_keys, 0)
    for copy in own_moves:
        copy.start()
    lax.fori_loop(0, groups, begin_values, 0)
    out_move.start()

    for copy in small:
        copy.wait()
    group = column(routes[:1, :]) // each
    down_at = lax.broadcasted_iota(jnp.int32, (count, count), 0)
    across = lax.broadcasted_iota(jnp.int32, (count, count), 1)
    other = routes[:1, :] // each
    before = jnp.where((group == other) & (across < down_at), 1, 0)
    target = group * height + jnp.sum(before, axis=1, keepdims=True)
    slots = zs * height
    chosen = target == lax.broadcasted_iota(jnp.int32, (count, slots), 1)
    chosen = jnp.where(chosen, 1.0, 0.0).astype(low)
    place = lax.broadcasted_iota(jnp.int32, (count, SIDE), 1)
    scale = jnp.zeros((count, SIDE), jnp.float32)
    for k in range(routes.shape[0]):
        inside = column(routes[k : k + 1, :]) - group * each
        scale += jnp.where(place == inside, column(route_weight[k : k + 1, :]), 0.0)
    high = scale.astype(low)
    side = jnp.concatenate([high, (scale - high.astype(jnp.float32)).astype(low)], axis=1)
    turned = (((0,), (0,)), ((), ()))
    packed = lax.dot_general(chosen, side, turned, preferred_element_type=jnp.float32)
    side_pack[...] = packed.astype(low).reshape(zs, height, 2 * SIDE)
    sides[0, y, x] = side_pack[z]

    entry = hidden[...].astype(jnp.float32)
    factor = lax.rsqrt(jnp.mean(entry * entry, axis=-1, keepdims=True) + epsilon)
    normed = (entry * factor * first_gain[...]).astype(low)
    lane = lax.broadcasted_iota(jnp.int32, (count, 2 * DK), 1)
    query_move.wait()
    query = jnp.dot(normed, query_buf[...], preferred_element_type=jnp.float32)
    query = query.astype(low).astype(jnp.float32)
    for head in range(HEADS):
        block = query[:, head * 2 * DK : (head + 1) * 2 * DK]
        queries[:, head, :] = jnp.where(lane < DK, block, 0.0)
        queries[:, HEADS + head, :] = jnp.where(lane < DK, 0.0, block)
    for index, result in ((0, new_key), (1, new_value)):
        kv_moves[index].wait()
        made = jnp.dot(normed, kv_buf[index], preferred_element_type=jnp.float32).astype(low)
        result[...] = made
        fresh[index] = made.astype(jnp.float32)

    pl.semaphore_wait(barrier, len(others) + 1)
    side_waits = {}
    for i, j, k in others:
        side_waits[i, j, k] = send(side_pack.at[zat(i)], sides.at[i, y, x], device(zat(i), yat(j), xat(k)))

    position = lax.broadcasted_iota(jnp.int32, (1, span), 1)
    mixes = column(mixing[...])

    def weigh(step, carry):
        fetch_keys(step).wait()
        for offset in range(batch):
            s = step * batch + offset
            wide = queries[s]
            own_key = fresh[0, pl.ds(s, 1), :]
            scores = lax.dot_general(
                wide.astype(low),
                key_buf[s],
                (((1,), (1,)), ((), ())),
                preferred_element_type=jnp.float32,
            ) * DK ** (-0.5)
            own = jnp.sum(wide * own_key, axis=-1, keepdims=True) * DK ** (-0.5)
            scores = jnp.where(position < lengths[s], scores, -jnp.inf)
            highest = jnp.maximum(jnp.max(scores, axis=-1, keepdims=True), own)
            weights = jnp.exp(scores - highest)
            own = jnp.exp(own - highest)
            inverse = 1.0 / (jnp.sum(weights, axis=-1, keepdims=True) + own)
            first, second = inverse[:HEADS], inverse[HEADS:] * mixes
            contrast[s] = weights[:HEADS] * first - weights[HEADS:] * second
            own = (own[:HEADS] * first - own[HEADS:] * second).astype(low).astype(jnp.float32)
            owns[s] = own * fresh[1, pl.ds(s, 1), :]
        return carry

    lax.fori_loop(0, groups, weigh, 0)

    pairs = ((gate, gate.at[0]), (up, up.at[0]), (down, down.at[0]))
    swaps = []
    for copy, (whole, mine) in zip(own_moves, pairs):
        copy.wait()
        swaps.append(send(mine, whole.at[1], sibling))

    def mix(step, carry):
        fetch_values(step).wait()
        for offset in range(batch):
            s = step * batch + offset
            mixed = jnp.dot(contrast[s].astype(low), value_buf[s], preferred_element_type=jnp.float32)
            mixed += owns[s]
            scale = lax.rsqrt(jnp.mean(mixed * mixed, axis=-1, keepdims=True) + epsilon)
            heads[s] = mixed * scale * head_gain[...]
        return carry

    lax.fori_loop(0, groups, mix, 0)

    joined = jnp.concatenate([heads[:, head, :] for head in range(HEADS)], axis=1).astype(low)
    out_move.wait()
    update = jnp.dot(joined, out_buf[...], preferred_element_type=jnp.float32)
    kept = (hidden[...].astype(jnp.float32) + update).astype(low)
    residual[...] = kept
    kept = kept.astype(jnp.float32)
    factor = lax.rsqrt(jnp.mean(kept * kept, axis=-1, keepdims=True) + epsilon)
    inputs = (kept * factor * second_gain[...]).astype(low)
    for h in range(2):
        packed = lax.dot_general(
            chosen, inputs[:, h * half : (h + 1) * half], turned, preferred_element_type=jnp.float32
        )
        pack[:, h] = packed.astype(low).reshape(zs, height, half)

    arrive, along_x, along_y, corner = {}, {}, {}, {}
    ones, twos, ends = {}, {}, {}

    def spread(i):
        if i:
            arrive[i].wait_recv()
        block = rows.at[i, y, x]
        corner[i] = []
        if i in STRAIGHT:
            for j in range(1, ys):
                for k in range(1, xs):
                    corner[i].append(send(block, block, device(z, yat(j), xat(k))))
        for j in range(1, xs):
            along_x[i, j] = send(block, block, device(z, y, xat(j)))
        for j in range(1, ys):
            along_y[i, j] = send(block, block, device(z, yat(j), x))

    def forward(i):
        if i in STRAIGHT:
            corner[i].extend(along_x.pop((i, j)) for j in range(1, xs))
            corner[i].extend(along_y.pop((i, j)) for j in range(1, ys))
            return
        for j in range(1, xs):
            along_x[i, j].wait_recv()
            block = rows.at[i, y, xat(-j), 0]
            for k in range(1, ys):
                corner[i].append(send(block, block, device(z, yat(k), x)))
        for j in range(1, ys):
            along_y[i, j].wait_recv()
            block = rows.at[i, yat(-j), x, 1]
            for k in range(1, xs):
                corner[i].append(send(block, block, device(z, y, xat(k))))

    spots = ys * xs
    spread_to = [(j, k) for j in range(ys) for k in range(xs) if j or k][::-1]
    mine_lane = y * xs + x
    seen = set()

    def wait_once(name, copies):
        if name not in seen:
            seen.add(name)
            for copy in copies:
                copy.wait_recv()

    def compute(i):
        for copy in corner[i]:
            copy.wait_recv()
        wait_once("swap", swaps[:2])
        for j in range(ys):
            for k in range(xs):
                if (i, j, k) in side_waits:
                    side_waits[i, j, k].wait_recv()
        flat = [rows[i, :, :, h].reshape(spots * height, half) for h in range(2)]
        side = sides[i].reshape(spots * height, 2 * SIDE).astype(jnp.float32)
        lane = lax.broadcasted_iota(jnp.int32, side.shape, 1)
        hit = lax.rem(lane, SIDE) == mine_lane
        scale = jnp.sum(jnp.where(hit, side, 0.0), axis=1, keepdims=True)
        inner = []
        for share in range(2):
            left = jnp.dot(flat[0], gate[share, :half], preferred_element_type=jnp.float32)
            left += jnp.dot(flat[1], gate[share, half:], preferred_element_type=jnp.float32)
            right = jnp.dot(flat[0], up[share, :half], preferred_element_type=jnp.float32)
            right += jnp.dot(flat[1], up[share, half:], preferred_element_type=jnp.float32)
            inner.append((left / (1.0 + jnp.exp(-left)) * right).astype(low))
        wait_once("down", swaps[2:])
        ones[i] = []
        tile = math.gcd(half, 512)
        for h in range(2):
            for start in range(0, half, tile):
                cols = slice(h * half + start, h * half + start + tile)
                total = jnp.dot(inner[0], down[0, :, cols], preferred_element_type=jnp.float32)
                total += jnp.dot(inner[1], down[1, :, cols], preferred_element_type=jnp.float32)
                total = (total * scale).astype(low).reshape(ys, xs, height, tile)
                if h == 0:
                    part_a[i, :, :, :, start : start + tile] = total
                else:
                    for k in range(xs):
                        part_b[i, k, :, :, start : start + tile] = total[:, k]
            if i in GATHER:
                if True:
                    push(i, h)
            elif h == 0:
                for j in range(1, ys):
                    ones[i].append(send(part_a.at[i, yat(j)], first_a.at[i, j - 1], device(z, yat(j), x)))
            else:
                for j in range(1, xs):
                    ones[i].append(send(part_b.at[i, xat(j)], first_b.at[i, j - 1], device(z, y, xat(j))))

    def push(i, h):
        for index, (j, k) in enumerate(spread_to):
            src = part_a.at[i, yat(j), xat(k)] if h == 0 else part_b.at[i, xat(k), yat(j)]
            ones[i].append(send(src, direct.at[i, index, h], device(z, yat(j), xat(k))))

    def push_both(i):
        for h in range(2):
            push(i, h)

    def reduce(i):
        if i in GATHER:
            return
        twos[i] = []
        for copy in ones[i][: ys - 1]:
            copy.wait_recv()
        for k in range(1, xs):
            total = part_a[i, y, xat(k)].astype(jnp.float32)
            for j in range(1, ys):
                total += first_a[i, j - 1, xat(k)].astype(jnp.float32)
            send_a[i, k - 1] = total.astype(low)
            twos[i].append(send(send_a.at[i, k - 1], second_a.at[i, k - 1], device(z, y, xat(k))))
        for copy in ones[i][ys - 1 :]:
            copy.wait_recv()
        for k in range(1, ys):
            total = part_b[i, x, yat(k)].astype(jnp.float32)
            for j in range(1, xs):
                total += first_b[i, j - 1, yat(k)].astype(jnp.float32)
            send_b[i, k - 1] = total.astype(low)
            twos[i].append(send(send_b.at[i, k - 1], second_b.at[i, k - 1], device(z, yat(k), x)))

    def settle(i):
        for h in range(2):
            if i in GATHER:
                for copy in ones[i][h * (spots - 1) : (h + 1) * (spots - 1)]:
                    copy.wait_recv()
                total = (part_a[i, y, x] if h == 0 else part_b[i, x, y]).astype(jnp.float32)
                for index in range(spots - 1):
                    total += direct[i, index, h].astype(jnp.float32)
            elif h == 0:
                for copy in twos[i][: xs - 1]:
                    copy.wait_recv()
                total = part_a[i, y, x].astype(jnp.float32)
                for j in range(1, ys):
                    total += first_a[i, j - 1, x].astype(jnp.float32)
                for k in range(1, xs):
                    total += second_a[i, k - 1].astype(jnp.float32)
            else:
                for copy in twos[i][xs - 1 :]:
                    copy.wait_recv()
                total = part_b[i, x, y].astype(jnp.float32)
                for j in range(1, xs):
                    total += first_b[i, j - 1, y].astype(jnp.float32)
                for k in range(1, ys):
                    total += second_b[i, k - 1].astype(jnp.float32)
            if i:
                final[i - 1, h] = total.astype(low)
                ends[i, h] = send(final.at[i - 1, h], back.at[z, h], device(zat(i), y, x))
            else:
                back[z, h] = total.astype(low)

    for i in (1, 2, 3):
        arrive[i] = send(pack.at[zat(i)], rows.at[i, y, x], device(zat(i), y, x))
    rows[0, y, x] = pack[z]
    stages = {"s": spread, "f": forward, "c": compute, "p": push_both, "r": reduce, "e": settle}
    for name in ORDER:
        stages[name[0]](int(name[1:]))
    for h in range(2):
        for i in range(1, zs):
            if (i, h) in ends:
                ends[i, h].wait_recv()
        filled = back[:, h].reshape(slots, half)
        routed = jnp.dot(chosen, filled, preferred_element_type=jnp.float32)
        cols = slice(h * half, (h + 1) * half)
        out[:, cols] = (residual[:, cols].astype(jnp.float32) + routed).astype(out.dtype)
    for copy in used:
        copy.wait_send()


def run_layer(arrays, own, devices):
    (hidden, cache_keys, cache_values, lengths, first_gain, query_weight, key_weight, value_weight,
     mixing, head_gain, out_weight, second_gain, routes, route_weight) = arrays
    count, width = hidden.shape
    span = cache_keys.shape[1]
    zs = GROUPS
    chips = devices // (2 * zs)
    xs = math.isqrt(chips)
    ys = chips // xs
    experts = devices // EXP_SPLIT
    each = experts // zs
    capacity = max(2, 2 * count * TOP_K // experts)
    height = capacity * each // TOP_K
    half = width // 2
    inner = own[0].shape[2]
    low = jnp.bfloat16
    batch = math.gcd(count, 16)
    groups = count // batch
    sends = zs * ys * xs - 1 + 3 + 3 * (zs - 1) + zs * 4 * xs * ys
    vmem = pl.BlockSpec(memory_space=pltpu.VMEM)
    anywhere = pl.BlockSpec(memory_space=pltpu.HBM)
    small = [
        hidden, first_gain.reshape(1, -1), mixing.reshape(1, -1), head_gain.reshape(1, -1),
        second_gain.reshape(1, -1), routes.T, route_weight.T,
    ]
    return pl.pallas_call(
        functools.partial(layer_kernel, (zs, ys, xs), height, each),
        out_shape=(
            pltpu.VMEM((count, width), low),
            pltpu.VMEM((count, 2 * DK), low),
            pltpu.VMEM((count, DV), low),
        ),
        in_specs=[pl.BlockSpec(memory_space=pltpu.SMEM)] + [anywhere] * 16,
        out_specs=(vmem,) * 3,
        scratch_shapes=[
            *(pltpu.VMEM(array.shape, array.dtype) for array in small),
            pltpu.VMEM(cache_keys.shape, low),
            pltpu.VMEM(cache_values.shape, low),
            pltpu.VMEM(query_weight.shape, low),
            pltpu.VMEM((2, *key_weight.shape), low),
            pltpu.VMEM(out_weight.shape, low),
            pltpu.VMEM((count, 2 * HEADS, 2 * DK), jnp.float32),
            pltpu.VMEM((count, HEADS, DV), jnp.float32),
            pltpu.VMEM((2, count, DV), jnp.float32),
            pltpu.VMEM((count, HEADS, span), jnp.float32),
            pltpu.VMEM((count, HEADS, DV), jnp.float32),
            pltpu.VMEM((zs, 2, height, half), low),
            pltpu.VMEM((zs, height, 2 * SIDE), low),
            pltpu.VMEM((count, width), low),
            pltpu.VMEM((zs, ys, xs, 2, height, half), low),
            pltpu.VMEM((zs, ys, xs, height, 2 * SIDE), low),
            pltpu.VMEM((zs, ys, xs, height, half), low),
            pltpu.VMEM((zs, xs, ys, height, half), low),
            pltpu.VMEM((zs, max(1, ys - 1), xs, height, half), low),
            pltpu.VMEM((zs, max(1, xs - 1), ys, height, half), low),
            pltpu.VMEM((zs, max(1, xs - 1), height, half), low),
            pltpu.VMEM((zs, max(1, ys - 1), height, half), low),
            pltpu.VMEM((zs, max(1, xs - 1), height, half), low),
            pltpu.VMEM((zs, max(1, ys - 1), height, half), low),
            pltpu.VMEM((zs, max(1, ys * xs - 1), 2, height, half), low),
            pltpu.VMEM((zs - 1, 2, height, half), low),
            pltpu.VMEM((zs, 2, height, half), low),
            pltpu.VMEM((2, width, inner), low),
            pltpu.VMEM((2, width, inner), low),
            pltpu.VMEM((2, inner, width), low),
            pltpu.SemaphoreType.DMA((14,)),
            pltpu.SemaphoreType.DMA((groups,)),
            pltpu.SemaphoreType.DMA((groups,)),
            pltpu.SemaphoreType.DMA((sends,)),
            pltpu.SemaphoreType.DMA((sends,)),
        ],
        compiler_params=pltpu.CompilerParams(
            collective_id=0, has_side_effects=True, vmem_limit_bytes=60 * 1024 * 1024
        ),
        name="layer",
    )(
        lengths, hidden, cache_keys, cache_values, small[1], query_weight, key_weight, value_weight,
        small[2], small[3], out_weight, small[4], small[5], small[6], *own,
    )


def finish_kernel(*refs):
    count = len(refs) // 2
    sources, targets, sems = refs[:count], refs[count:-1], refs[-1]
    copies = [
        pltpu.make_async_copy(source, target, sems.at[index])
        for index, (source, target) in enumerate(zip(sources, targets))
    ]
    for copy in copies:
        copy.start()
    for copy in copies:
        copy.wait()


def finish(made):
    anywhere = pl.BlockSpec(memory_space=pl.ANY)
    return pl.pallas_call(
        finish_kernel,
        out_shape=tuple(jax.ShapeDtypeStruct(array.shape, array.dtype) for array in made),
        in_specs=[pl.BlockSpec(memory_space=pltpu.VMEM)] * len(made),
        out_specs=(anywhere,) * len(made),
        scratch_shapes=[pltpu.SemaphoreType.DMA((len(made),))],
        name="finish",
    )(*made)


def per_device(
    hidden,
    cache_keys,
    cache_values,
    lengths,
    first_gain,
    query_weight,
    key_weight,
    value_weight,
    mixing,
    head_gain,
    out_weight,
    second_gain,
    routes,
    route_weight,
    expert_gate,
    expert_up,
    expert_down,
):
    arrays = (
        hidden, cache_keys, cache_values, lengths, first_gain, query_weight, key_weight, value_weight,
        mixing, head_gain, out_weight, second_gain, routes, route_weight,
    )
    own = (expert_gate, expert_up, expert_down)
    made = run_layer(arrays, own, lax.axis_size("ep"))
    return finish([pltpu.with_memory_space_constraint(array, pltpu.VMEM) for array in made])


def solution(mesh):
    return jax.shard_map(
        per_device,
        mesh=mesh,
        in_specs=(
            P("ep", None),
            P("ep", None, None),
            P("ep", None, None),
            P("ep"),
            P(),
            P(),
            P(),
            P(),
            P(),
            P(),
            P(),
            P(),
            P("ep", None),
            P("ep", None),
            P("ep", None, None),
            P("ep", None, None),
            P("ep", None, None),
        ),
        out_specs=(P("ep", None), P("ep", None), P("ep", None)),
        check_vma=False,
    )
```

time: 56.2 us -> 44.5 us (0.79)
  Pallas kernels: 52.7 us -> 43.7 us
  local copies, waits for them, and re-layouts: 1.57 us -> 0 us
  starting transfers between devices: 1.07 us -> 0 us
    pallas_call x2, Pallas kernels: 52.7 us -> 43.7 us  [the longest x1 43 us: run_layer(): pl.pallas_call(functools.partial(layer_kernel, (zs, ys, xs), height, each...]
    unnamed x1 -> x0, local copies, waits for them, and re-layouts: 1.57 us -> none
    ppermute x3 -> x0, starting transfers between devices: 1.07 us -> none  [per_device(): other = tuple((lax.ppermute(array, 'ep', swap) for array in own))]
  transfers between devices with their start and end apart: 3 -> 0, of which waited for: 0 -> 0; matrix products, arithmetic and copies ran while one was open for 0% -> 0% of each run, Pallas kernels for 21% -> 0%
where the time goes in v2:
time: 44.5 us; the launch traced here: 44.3 us
  Pallas kernels  43.7 us (98%)
  between operations  0.65 us (1%)
    pallas_call x1, Pallas kernels, run_layer(): pl.pallas_call(functools.partial(layer_kernel, (zs, ys, xs), height, each...  43 us

profile of v2, /device:TPU:0, one launch (start us, length us, event | category | flops | bytes accessed | tf_op | source)
XLA Modules:
  0.0 44.3 jit_solution(11330768941565556188)
XLA Ops:
  0.6 43.0 %layer.1 = (bf16[32,2048]{1,0:T(8,128)(2,1)S(1)}, bf16[32,128]{1,0:T(8,128)(2,1)S(1)}, bf16[32,128]{1,0:T(8,128)(2,1)S(1)}) custom-call(s32[32]{0:T(128)} %lengths.1, bf16[32,2048]{1,0:T(8,128)(2,1)} %hidden_in.1, bf16[32,1024,128]{2,1,0:T(8,128)(2,1)} %keys.1, bf16[32,1024,128]{2,1,0:T(8,128)(2,1)} %values.1, f32[1,2048]{1,0:T(1,128)} %bitcast.6, ...), custom_call_target="tpu_custom_call" | custom-call | tf_op jit(solution)/shard_map/layer/pallas_call | solution.py:434
  43.6 0.7 %finish.1 = (bf16[32,2048]{1,0:T(8,128)(2,1)}, bf16[32,128]{1,0:T(8,128)(2,1)}, bf16[32,128]{1,0:T(8,128)(2,1)}) custom-call(bf16[32,2048]{1,0:T(8,128)(2,1)S(1)} %get-tuple-element.6.refs_0_, bf16[32,128]{1,0:T(8,128)(2,1)S(1)} %get-tuple-element.7.refs_1_, bf16[32,128]{1,0:T(8,128)(2,1)S(1)} %get-tuple-element.8.refs_2_), custom_call_target="tpu_custom_call" | custom-call | tf_op jit(solution)/shard_map/finish/pallas_call | solution.py:505

commit v3 on v2

--- a/solution.py
+++ b/solution.py
@@ -16,9 +16,8 @@
 TOP_K = 4
 GROUPS = 4
 SIDE = 64
-ORDER = ('s0', 'f0', 's1', 'f1', 's2', 'f2', 's3', 'f3', 'c2', 'c3', 'e2', 'c1', 'e3', 'c0', 'e1', 'e0')
-STRAIGHT = (0, 1, 2, 3)
-GATHER = (0, 1, 2, 3)
+ORDER = ('s0', 's1', 'w0', 's2', 's3', 's6', 's7', 's4', 's5', 'c3', 'c2', 'e3', 'c1', 'e2', 'c0', 'e1', 'e0')
+PIECE = 512
 
 
 epsilon = 1e-06
@@ -31,14 +30,13 @@
     return jnp.sum(jnp.where(down == across, row, jnp.zeros_like(row)), axis=1, keepdims=True)
 
 
-def layer_kernel(dims, height, each, lengths, hidden_in, keys, values, first_gain_in, query_weight, key_weight,
+def layer_kernel(dims, height, each, lengths_in, hidden_in, keys, values, first_gain_in, query_weight, key_weight,
                  value_weight, mixing_in, head_gain_in, out_weight, second_gain_in, routes_in, route_weight_in,
                  gate_own, up_own, down_own,
                  out, new_key, new_value,
                  hidden, first_gain, mixing, head_gain, second_gain, routes, route_weight,
-                 key_buf, value_buf, query_buf, kv_buf, out_buf, queries, heads, fresh, contrast, owns,
-                 pack, side_pack, residual, rows, sides, part_a, part_b, first_a, first_b, send_a, send_b,
-                 second_a, second_b, direct, final, back, gate, up, down,
+                 lengths, key_buf, value_buf, query_buf, kv_buf, out_buf, queries, heads, fresh, contrast, owns,
+                 pack, side_pack, residual, rows, sides, part, direct, final, back, gate, up, down,
                  load_sems, key_sems, value_sems, send_sems, recv_sems):
     zs, ys, xs = dims
     count, width = hidden.shape
@@ -86,6 +84,50 @@
         used.append(copy)
         return copy
 
+    moves = []
+    for src, dst in (
+        (hidden_in, hidden), (first_gain_in, first_gain), (routes_in, routes), (route_weight_in, route_weight),
+        (mixing_in, mixing), (head_gain_in, head_gain), (second_gain_in, second_gain), (lengths_in, lengths),
+        (query_weight, query_buf), (key_weight, kv_buf.at[0]), (value_weight, kv_buf.at[1]),
+        (gate_own.at[0], gate.at[0]), (up_own.at[0], up.at[0]), (down_own.at[0], down.at[0]),
+    ):
+        moves.append(pltpu.make_async_copy(src, dst, load_sems.at[len(moves)]))
+    small, query_move, kv_moves, own_moves = moves[:8], moves[8], moves[9:11], moves[11:]
+    piece = math.gcd(width, PIECE)
+    out_moves = [
+        pltpu.make_async_copy(
+            out_weight.at[:, pl.ds(start, piece)], out_buf.at[:, pl.ds(start, piece)],
+            load_sems.at[len(moves) + start // piece],
+        )
+        for start in range(0, width, piece)
+    ]
+
+    def fetch(source, target, flags, step):
+        at = pl.ds(step * batch, batch)
+        return pltpu.make_async_copy(source.at[at], target.at[at], flags.at[step])
+
+    def fetch_keys(step):
+        return fetch(keys, key_buf, key_sems, step)
+
+    def fetch_values(step):
+        return fetch(values, value_buf, value_sems, step)
+
+    for copy in (*small, query_move, *kv_moves):
+        copy.start()
+
+    def begin_keys(step, carry):
+        fetch_keys(step).start()
+        return carry
+
+    def begin_values(step, carry):
+        fetch_values(step).start()
+        return carry
+
+    lax.fori_loop(0, groups, begin_keys, 0)
+    lax.fori_loop(0, groups, begin_values, 0)
+    for copy in (*out_moves, *own_moves):
+        copy.start()
+
     others = [
         (i, j, k) for i in range(zs) for j in range(ys) for k in range(xs) if (i, j, k) != (0, 0, 0)
     ]
@@ -96,43 +138,6 @@
             barrier, inc=1, device_id=(device(zat(i), yat(j), xat(k)),), device_id_type=pl.DeviceIdType.MESH
         )
     pl.semaphore_signal(barrier, inc=1, device_id=(sibling,), device_id_type=pl.DeviceIdType.MESH)
-
-    moves = []
-    for src, dst in (
-        (hidden_in, hidden), (first_gain_in, first_gain), (routes_in, routes), (route_weight_in, route_weight),
-        (mixing_in, mixing), (head_gain_in, head_gain), (second_gain_in, second_gain),
-        (query_weight, query_buf), (key_weight, kv_buf.at[0]), (value_weight, kv_buf.at[1]),
-        (out_weight, out_buf), (gate_own.at[0], gate.at[0]), (up_own.at[0], up.at[0]), (down_own.at[0], down.at[0]),
-    ):
-        moves.append(pltpu.make_async_copy(src, dst, load_sems.at[len(moves)]))
-    small, query_move, kv_moves, out_move, own_moves = moves[:7], moves[7], moves[8:10], moves[10], moves[11:]
-
-    def fetch(source, target, flags, step):
-        at = pl.ds(step * batch, batch)
-        return pltpu.make_async_copy(source.at[at], target.at[at], flags.at[step])
-
-    def fetch_keys(step):
-        return fetch(keys, key_buf, key_sems, step)
-
-    def fetch_values(step):
-        return fetch(values, value_buf, value_sems, step)
-
-    for copy in (*small, query_move, *kv_moves):
-        copy.start()
-
-    def begin_keys(step, carry):
-        fetch_keys(step).start()
-        return carry
-
-    def begin_values(step, carry):
-        fetch_values(step).start()
-        return carry
-
-    lax.fori_loop(0, groups, begin_keys, 0)
-    for copy in own_moves:
-        copy.start()
-    lax.fori_loop(0, groups, begin_values, 0)
-    out_move.start()
 
     for copy in small:
         copy.wait()
@@ -173,11 +178,6 @@
         made = jnp.dot(normed, kv_buf[index], preferred_element_type=jnp.float32).astype(low)
         result[...] = made
         fresh[index] = made.astype(jnp.float32)
-
-    pl.semaphore_wait(barrier, len(others) + 1)
-    side_waits = {}
-    for i, j, k in others:
-        side_waits[i, j, k] = send(side_pack.at[zat(i)], sides.at[i, y, x], device(zat(i), yat(j), xat(k)))
 
     position = lax.broadcasted_iota(jnp.int32, (1, span), 1)
     mixes = column(mixing[...])
@@ -208,11 +208,10 @@
 
     lax.fori_loop(0, groups, weigh, 0)
 
-    pairs = ((gate, gate.at[0]), (up, up.at[0]), (down, down.at[0]))
-    swaps = []
-    for copy, (whole, mine) in zip(own_moves, pairs):
-        copy.wait()
-        swaps.append(send(mine, whole.at[1], sibling))
+    pl.semaphore_wait(barrier, len(others) + 1)
+    side_waits = {}
+    for i, j, k in others:
+        side_waits[i, j, k] = send(side_pack.at[zat(i)], sides.at[i, y, x], device(zat(i), yat(j), xat(k)))
 
     def mix(step, carry):
         fetch_values(step).wait()
@@ -227,11 +226,12 @@
     lax.fori_loop(0, groups, mix, 0)
 
     joined = jnp.concatenate([heads[:, head, :] for head in range(HEADS)], axis=1).astype(low)
-    out_move.wait()
-    update = jnp.dot(joined, out_buf[...], preferred_element_type=jnp.float32)
-    kept = (hidden[...].astype(jnp.float32) + update).astype(low)
-    residual[...] = kept
-    kept = kept.astype(jnp.float32)
+    for index, copy in enumerate(out_moves):
+        cols = slice(index * piece, (index + 1) * piece)
+        copy.wait()
+        update = jnp.dot(joined, out_buf[:, cols], preferred_element_type=jnp.float32)
+        residual[:, cols] = (hidden[:, cols].astype(jnp.float32) + update).astype(low)
+    kept = residual[...].astype(jnp.float32)
     factor = lax.rsqrt(jnp.mean(kept * kept, axis=-1, keepdims=True) + epsilon)
     inputs = (kept * factor * second_gain[...]).astype(low)
     for h in range(2):
@@ -240,43 +240,17 @@
         )
         pack[:, h] = packed.astype(low).reshape(zs, height, half)
 
-    arrive, along_x, along_y, corner = {}, {}, {}, {}
-    ones, twos, ends = {}, {}, {}
-
-    def spread(i):
-        if i:
-            arrive[i].wait_recv()
-        block = rows.at[i, y, x]
-        corner[i] = []
-        if i in STRAIGHT:
-            for j in range(1, ys):
-                for k in range(1, xs):
-                    corner[i].append(send(block, block, device(z, yat(j), xat(k))))
-        for j in range(1, xs):
-            along_x[i, j] = send(block, block, device(z, y, xat(j)))
-        for j in range(1, ys):
-            along_y[i, j] = send(block, block, device(z, yat(j), x))
-
-    def forward(i):
-        if i in STRAIGHT:
-            corner[i].extend(along_x.pop((i, j)) for j in range(1, xs))
-            corner[i].extend(along_y.pop((i, j)) for j in range(1, ys))
-            return
-        for j in range(1, xs):
-            along_x[i, j].wait_recv()
-            block = rows.at[i, y, xat(-j), 0]
-            for k in range(1, ys):
-                corner[i].append(send(block, block, device(z, yat(k), x)))
-        for j in range(1, ys):
-            along_y[i, j].wait_recv()
-            block = rows.at[i, yat(-j), x, 1]
-            for k in range(1, xs):
-                corner[i].append(send(block, block, device(z, y, xat(k))))
-
+    arrive, spread_waits, gather_waits, ends = {}, {}, {}, {}
     spots = ys * xs
     spread_to = [(j, k) for j in range(ys) for k in range(xs) if j or k][::-1]
     mine_lane = y * xs + x
+    swaps = []
     seen = set()
+
+    def swap(_):
+        for copy, (whole, mine) in zip(own_moves, ((gate, gate.at[0]), (up, up.at[0]), (down, down.at[0]))):
+            copy.wait()
+            swaps.append(send(mine, whole.at[1], sibling))
 
     def wait_once(name, copies):
         if name not in seen:
@@ -284,9 +258,17 @@
             for copy in copies:
                 copy.wait_recv()
 
+    def spread(code):
+        i, h = divmod(code, 2)
+        if i:
+            arrive[i, h].wait_recv()
+        block = rows.at[i, y, x, h]
+        spread_waits[i, h] = [send(block, block, device(z, yat(j), xat(k))) for j, k in spread_to]
+
     def compute(i):
-        for copy in corner[i]:
-            copy.wait_recv()
+        for h in range(2):
+            for copy in spread_waits[i, h]:
+                copy.wait_recv()
         wait_once("swap", swaps[:2])
         for j in range(ys):
             for k in range(xs):
@@ -305,7 +287,6 @@
             right += jnp.dot(flat[1], up[share, half:], preferred_element_type=jnp.float32)
             inner.append((left / (1.0 + jnp.exp(-left)) * right).astype(low))
         wait_once("down", swaps[2:])
-        ones[i] = []
         tile = math.gcd(half, 512)
         for h in range(2):
             for start in range(0, half, tile):
@@ -313,91 +294,35 @@
                 total = jnp.dot(inner[0], down[0, :, cols], preferred_element_type=jnp.float32)
                 total += jnp.dot(inner[1], down[1, :, cols], preferred_element_type=jnp.float32)
                 total = (total * scale).astype(low).reshape(ys, xs, height, tile)
-                if h == 0:
-                    part_a[i, :, :, :, start : start + tile] = total
-                else:
-                    for k in range(xs):
-                        part_b[i, k, :, :, start : start + tile] = total[:, k]
-            if i in GATHER:
-                if True:
-                    push(i, h)
-            elif h == 0:
-                for j in range(1, ys):
-                    ones[i].append(send(part_a.at[i, yat(j)], first_a.at[i, j - 1], device(z, yat(j), x)))
-            else:
-                for j in range(1, xs):
-                    ones[i].append(send(part_b.at[i, xat(j)], first_b.at[i, j - 1], device(z, y, xat(j))))
-
-    def push(i, h):
-        for index, (j, k) in enumerate(spread_to):
-            src = part_a.at[i, yat(j), xat(k)] if h == 0 else part_b.at[i, xat(k), yat(j)]
-            ones[i].append(send(src, direct.at[i, index, h], device(z, yat(j), xat(k))))
-
-    def push_both(i):
-        for h in range(2):
-            push(i, h)
-
-    def reduce(i):
-        if i in GATHER:
-            return
-        twos[i] = []
-        for copy in ones[i][: ys - 1]:
-            copy.wait_recv()
-        for k in range(1, xs):
-            total = part_a[i, y, xat(k)].astype(jnp.float32)
-            for j in range(1, ys):
-                total += first_a[i, j - 1, xat(k)].astype(jnp.float32)
-            send_a[i, k - 1] = total.astype(low)
-            twos[i].append(send(send_a.at[i, k - 1], second_a.at[i, k - 1], device(z, y, xat(k))))
-        for copy in ones[i][ys - 1 :]:
-            copy.wait_recv()
-        for k in range(1, ys):
-            total = part_b[i, x, yat(k)].astype(jnp.float32)
-            for j in range(1, xs):
-                total += first_b[i, j - 1, yat(k)].astype(jnp.float32)
-            send_b[i, k - 1] = total.astype(low)
-            twos[i].append(send(send_b.at[i, k - 1], second_b.at[i, k - 1], device(z, yat(k), x)))
+                part[i, h, :, :, :, start : start + tile] = total
+            gather_waits[i, h] = [
+                send(part.at[i, h, yat(j), xat(k)], direct.at[i, h, index], device(z, yat(j), xat(k)))
+                for index, (j, k) in enumerate(spread_to)
+            ]
 
     def settle(i):
         for h in range(2):
-            if i in GATHER:
-                for copy in ones[i][h * (spots - 1) : (h + 1) * (spots - 1)]:
-                    copy.wait_recv()
-                total = (part_a[i, y, x] if h == 0 else part_b[i, x, y]).astype(jnp.float32)
-                for index in range(spots - 1):
-                    total += direct[i, index, h].astype(jnp.float32)
-            elif h == 0:
-                for copy in twos[i][: xs - 1]:
-                    copy.wait_recv()
-                total = part_a[i, y, x].astype(jnp.float32)
-                for j in range(1, ys):
-                    total += first_a[i, j - 1, x].astype(jnp.float32)
-                for k in range(1, xs):
-                    total += second_a[i, k - 1].astype(jnp.float32)
-            else:
-                for copy in twos[i][xs - 1 :]:
-                    copy.wait_recv()
-                total = part_b[i, x, y].astype(jnp.float32)
-                for j in range(1, xs):
-                    total += first_b[i, j - 1, y].astype(jnp.float32)
-                for k in range(1, ys):
-                    total += second_b[i, k - 1].astype(jnp.float32)
+            for copy in gather_waits[i, h]:
+                copy.wait_recv()
+            total = part[i, h, y, x].astype(jnp.float32)
+            for index in range(spots - 1):
+                total += direct[i, h, index].astype(jnp.float32)
             if i:
                 final[i - 1, h] = total.astype(low)
                 ends[i, h] = send(final.at[i - 1, h], back.at[z, h], device(zat(i), y, x))
             else:
                 back[z, h] = total.astype(low)
 
-    for i in (1, 2, 3):
-        arrive[i] = send(pack.at[zat(i)], rows.at[i, y, x], device(zat(i), y, x))
+    for i, h in ((1, 0), (1, 1), (3, 0), (3, 1), (2, 0), (2, 1)):
+        if i:
+            arrive[i, h] = send(pack.at[zat(i), h], rows.at[i, y, x, h], device(zat(i), y, x))
     rows[0, y, x] = pack[z]
-    stages = {"s": spread, "f": forward, "c": compute, "p": push_both, "r": reduce, "e": settle}
+    stages = {"w": swap, "s": spread, "c": compute, "e": settle}
     for name in ORDER:
         stages[name[0]](int(name[1:]))
     for h in range(2):
         for i in range(1, zs):
-            if (i, h) in ends:
-                ends[i, h].wait_recv()
+            ends[i, h].wait_recv()
         filled = back[:, h].reshape(slots, half)
         routed = jnp.dot(chosen, filled, preferred_element_type=jnp.float32)
         cols = slice(h * half, (h + 1) * half)
@@ -424,7 +349,7 @@
     low = jnp.bfloat16
     batch = math.gcd(count, 16)
     groups = count // batch
-    sends = zs * ys * xs - 1 + 3 + 3 * (zs - 1) + zs * 4 * xs * ys
+    sends = zs * ys * xs - 1 + 3 + 4 * (zs - 1) + 4 * zs * (ys * xs - 1)
     vmem = pl.BlockSpec(memory_space=pltpu.VMEM)
     anywhere = pl.BlockSpec(memory_space=pltpu.HBM)
     small = [
@@ -438,10 +363,11 @@
             pltpu.VMEM((count, 2 * DK), low),
             pltpu.VMEM((count, DV), low),
         ),
-        in_specs=[pl.BlockSpec(memory_space=pltpu.SMEM)] + [anywhere] * 16,
+        in_specs=[anywhere] * 17,
         out_specs=(vmem,) * 3,
         scratch_shapes=[
             *(pltpu.VMEM(array.shape, array.dtype) for array in small),
+            pltpu.SMEM(lengths.shape, lengths.dtype),
             pltpu.VMEM(cache_keys.shape, low),
             pltpu.VMEM(cache_values.shape, low),
             pltpu.VMEM(query_weight.shape, low),
@@ -457,21 +383,14 @@
             pltpu.VMEM((count, width), low),
             pltpu.VMEM((zs, ys, xs, 2, height, half), low),
             pltpu.VMEM((zs, ys, xs, height, 2 * SIDE), low),
-            pltpu.VMEM((zs, ys, xs, height, half), low),
-            pltpu.VMEM((zs, xs, ys, height, half), low),
-            pltpu.VMEM((zs, max(1, ys - 1), xs, height, half), low),
-            pltpu.VMEM((zs, max(1, xs - 1), ys, height, half), low),
-            pltpu.VMEM((zs, max(1, xs - 1), height, half), low),
-            pltpu.VMEM((zs, max(1, ys - 1), height, half), low),
-            pltpu.VMEM((zs, max(1, xs - 1), height, half), low),
-            pltpu.VMEM((zs, max(1, ys - 1), height, half), low),
-            pltpu.VMEM((zs, max(1, ys * xs - 1), 2, height, half), low),
+            pltpu.VMEM((zs, 2, ys, xs, height, half), low),
+            pltpu.VMEM((zs, 2, max(1, ys * xs - 1), height, half), low),
             pltpu.VMEM((zs - 1, 2, height, half), low),
             pltpu.VMEM((zs, 2, height, half), low),
             pltpu.VMEM((2, width, inner), low),
             pltpu.VMEM((2, width, inner), low),
             pltpu.VMEM((2, inner, width), low),
-            pltpu.SemaphoreType.DMA((14,)),
+            pltpu.SemaphoreType.DMA((14 + width // math.gcd(width, PIECE),)),
             pltpu.SemaphoreType.DMA((groups,)),
             pltpu.SemaphoreType.DMA((groups,)),
             pltpu.SemaphoreType.DMA((sends,)),

time: 44.5 us -> 42.2 us (0.948)
  Pallas kernels: 43.7 us -> 41.4 us
    pallas_call x1, Pallas kernels: 43 us -> 40.7 us  [run_layer(): pl.pallas_call(functools.partial(layer_kernel, (zs, ys, xs), height, each...]
where the time goes in v3:
time: 42.2 us; the launch traced here: 42.1 us
  Pallas kernels  41.4 us (98%)
  between operations  0.65 us (2%)
    pallas_call x1, Pallas kernels, run_layer(): pl.pallas_call(functools.partial(layer_kernel, (zs, ys, xs), height, each...  40.7 us

profile of v3, /device:TPU:0, one launch (start us, length us, event | category | flops | bytes accessed | tf_op | source)
XLA Modules:
  0.0 42.1 jit_solution(11354021590528540956)
XLA Ops:
  0.6 40.7 %layer.1 = (bf16[32,2048]{1,0:T(8,128)(2,1)S(1)}, bf16[32,128]{1,0:T(8,128)(2,1)S(1)}, bf16[32,128]{1,0:T(8,128)(2,1)S(1)}) custom-call(s32[32]{0:T(128)} %lengths_in.1, bf16[32,2048]{1,0:T(8,128)(2,1)} %hidden_in.1, bf16[32,1024,128]{2,1,0:T(8,128)(2,1)} %keys.1, bf16[32,1024,128]{2,1,0:T(8,128)(2,1)} %values.1, f32[1,2048]{1,0:T(1,128)} %bitcast.6, ...), custom_call_target="tpu_custom_call" | custom-call | tf_op jit(solution)/shard_map/layer/pallas_call | solution.py:359
  41.4 0.7 %finish.1 = (bf16[32,2048]{1,0:T(8,128)(2,1)}, bf16[32,128]{1,0:T(8,128)(2,1)}, bf16[32,128]{1,0:T(8,128)(2,1)}) custom-call(bf16[32,2048]{1,0:T(8,128)(2,1)S(1)} %get-tuple-element.6.refs_0_, bf16[32,128]{1,0:T(8,128)(2,1)S(1)} %get-tuple-element.7.refs_1_, bf16[32,128]{1,0:T(8,128)(2,1)S(1)} %get-tuple-element.8.refs_2_), custom_call_target="tpu_custom_call" | custom-call | tf_op jit(solution)/shard_map/finish/pallas_call | solution.py:424

commit v4 on v3

--- a/solution.py
+++ b/solution.py
@@ -17,7 +17,7 @@
 GROUPS = 4
 SIDE = 64
 ORDER = ('s0', 's1', 'w0', 's2', 's3', 's6', 's7', 's4', 's5', 'c3', 'c2', 'e3', 'c1', 'e2', 'c0', 'e1', 'e0')
-PIECE = 512
+PIECE = 1024
 
 
 epsilon = 1e-06
@@ -103,7 +103,8 @@
     ]
 
     def fetch(source, target, flags, step):
-        at = pl.ds(step * batch, batch)
+        size = count // flags.shape[0]
+        at = pl.ds(step * size, size)
         return pltpu.make_async_copy(source.at[at], target.at[at], flags.at[step])
 
     def fetch_keys(step):
@@ -124,7 +125,7 @@
         return carry
 
     lax.fori_loop(0, groups, begin_keys, 0)
-    lax.fori_loop(0, groups, begin_values, 0)
+    lax.fori_loop(0, value_sems.shape[0], begin_values, 0)
     for copy in (*out_moves, *own_moves):
         copy.start()
 
@@ -215,15 +216,16 @@
 
     def mix(step, carry):
         fetch_values(step).wait()
-        for offset in range(batch):
-            s = step * batch + offset
+        size = count // value_sems.shape[0]
+        for offset in range(size):
+            s = step * size + offset
             mixed = jnp.dot(contrast[s].astype(low), value_buf[s], preferred_element_type=jnp.float32)
             mixed += owns[s]
             scale = lax.rsqrt(jnp.mean(mixed * mixed, axis=-1, keepdims=True) + epsilon)
             heads[s] = mixed * scale * head_gain[...]
         return carry
 
-    lax.fori_loop(0, groups, mix, 0)
+    lax.fori_loop(0, value_sems.shape[0], mix, 0)
 
     joined = jnp.concatenate([heads[:, head, :] for head in range(HEADS)], axis=1).astype(low)
     for index, copy in enumerate(out_moves):
@@ -392,7 +394,7 @@
             pltpu.VMEM((2, inner, width), low),
             pltpu.SemaphoreType.DMA((14 + width // math.gcd(width, PIECE),)),
             pltpu.SemaphoreType.DMA((groups,)),
-            pltpu.SemaphoreType.DMA((groups,)),
+            pltpu.SemaphoreType.DMA((count // math.gcd(count, 16),)),
             pltpu.SemaphoreType.DMA((sends,)),
             pltpu.SemaphoreType.DMA((sends,)),
         ],

time: 42.2 us -> 42 us (level)
  no operation moved by 1% of the time
where the time goes in v4:
time: 42 us; the launch traced here: 41.9 us
  Pallas kernels  41.2 us (98%)
  between operations  0.65 us (2%)
    pallas_call x1, Pallas kernels, run_layer(): pl.pallas_call(functools.partial(layer_kernel, (zs, ys, xs), height, each...  40.6 us

profile of v4, /device:TPU:0, one launch (start us, length us, event | category | flops | bytes accessed | tf_op | source)
XLA Modules:
  0.0 41.9 jit_solution(17669846504322521103)
XLA Ops:
  0.6 40.6 %layer.1 = (bf16[32,2048]{1,0:T(8,128)(2,1)S(1)}, bf16[32,128]{1,0:T(8,128)(2,1)S(1)}, bf16[32,128]{1,0:T(8,128)(2,1)S(1)}) custom-call(s32[32]{0:T(128)} %lengths_in.1, bf16[32,2048]{1,0:T(8,128)(2,1)} %hidden_in.1, bf16[32,1024,128]{2,1,0:T(8,128)(2,1)} %keys.1, bf16[32,1024,128]{2,1,0:T(8,128)(2,1)} %values.1, f32[1,2048]{1,0:T(1,128)} %bitcast.6, ...), custom_call_target="tpu_custom_call" | custom-call | tf_op jit(solution)/shard_map/layer/pallas_call | solution.py:361
  41.2 0.7 %finish.1 = (bf16[32,2048]{1,0:T(8,128)(2,1)}, bf16[32,128]{1,0:T(8,128)(2,1)}, bf16[32,128]{1,0:T(8,128)(2,1)}) custom-call(bf16[32,2048]{1,0:T(8,128)(2,1)S(1)} %get-tuple-element.6.refs_0_, bf16[32,128]{1,0:T(8,128)(2,1)S(1)} %get-tuple-element.7.refs_1_, bf16[32,128]{1,0:T(8,128)(2,1)S(1)} %get-tuple-element.8.refs_2_), custom_call_target="tpu_custom_call" | custom-call | tf_op jit(solution)/shard_map/finish/pallas_call | solution.py:426
